TPU v7x, 32 devices: a whole 2x2x4 slice. The times are simulated.
32 devices in a mesh: sp: 8 (over z, x), tp: 4 (over y, core).
Axes of the slice: x: 2, y: 2, z: 4, core: 2. Of those that a mesh axis runs over, the one named last changes fastest.
Arguments:
- tokens: bfloat16 [6144, 2048], P('sp', 'tp'), may hold values from -23 to 23, as said below
- norm_gain: float32 [2048], replicated, may hold values from 0.8 to 8, as said below
- window_query: bfloat16 [2048, 1024], P(None, 'tp'), may hold values from -0.125 to 0.125
- window_key: bfloat16 [2048, 512], P(None, 'tp'), may hold values from -0.125 to 0.125
- window_value: bfloat16 [2048, 512], P(None, 'tp'), may hold values from -0.125 to 0.125
- sink_logit: float32 [16], P('tp'), may hold values from 2 to 6
- down_query: bfloat16 [2048, 768], replicated, may hold values from -0.125 to 0.125
- down_latent: bfloat16 [2048, 512], replicated, may hold values from -0.125 to 0.125
- rotary_proj: bfloat16 [2048, 32], replicated, may hold values from -0.125 to 0.125
- query_gain: float32 [768], replicated, may hold values from 0.8 to 8, as said below
- latent_gain: float32 [512], replicated, may hold values from 0.8 to 8, as said below
- up_query: bfloat16 [768, 1536], P(None, 'tp'), may hold values from -0.21875 to 0.21875
- up_key: bfloat16 [512, 1024], P(None, 'tp'), may hold values from -0.25 to 0.25
- up_value: bfloat16 [512, 1024], P(None, 'tp'), may hold values from -0.25 to 0.25
- window_out: bfloat16 [1024, 2048], P('tp'), may hold values from -0.125 to 0.125
- latent_out: bfloat16 [1024, 2048], P('tp'), may hold values from -0.125 to 0.125
Outputs:
- mixed: bfloat16 [6144, 2048], P(('sp', 'tp'))
Inputs may be any that keep to these rules, and one draw needn't show every extreme that they name: `tokens`: real-valued; the channels carry scales that vary smoothly by a factor of up to twenty across the width. `norm_gain`: positive. `query_gain`: positive. `latent_gain`: positive.
All inputs are finite; a program needn't handle non-finite values.
Results may differ from a plain program's by a relative error of at most 0.04.
The roundings to bfloat16 on the way count: a program that leaves them out, or rounds other values in their place, can miss the bound.
Values may be sent and summed in bfloat16 or wider, within the bound.
A program may use at most 128 MiB of HBM per device.

v0:
```python
import jax
import jax.numpy as jnp
from jax import lax
from jax.sharding import PartitionSpec as P

D = 2048
A_HEADS = 16
HD = 64
NOPE = 64
ROPE = 32
VD = 64
WINDOW = 128
QBLOCK = 256


EPS = 1e-06
THETA = 10000.0
key_span = 1024


def with_halo(x, sides, width):
    for axis, dim in sides:
        size, length = (lax.axis_size(axis), x.shape[dim])
        up = [(i, (i + 1) % size) for i in range(size - 1)]
        down = [(j, i) for i, j in up]
        last = lax.slice_in_dim(x, length - width, length, axis=dim)
        initial = lax.slice_in_dim(x, 0, width, axis=dim)
        before = lax.ppermute(last, axis, up)
        after = lax.ppermute(initial, axis, down)
        x = jnp.concatenate([before, x, after], axis=dim)
    return x


def rotate(vector, positions):
    half_len = vector.shape[-1] // 2
    inverse = THETA ** (-jnp.arange(half_len, dtype=jnp.float32) / half_len)
    angles = positions.astype(jnp.float32)[:, None] * inverse[None, :]
    new_shape = (angles.shape[0],) + (1,) * (vector.ndim - 2) + (half_len,)
    cosine = jnp.cos(angles).reshape(new_shape)
    sine_part = jnp.sin(angles).reshape(new_shape)
    front_half = vector[..., :half_len].astype(jnp.float32)
    second = vector[..., half_len:].astype(jnp.float32)
    return jnp.concatenate(
        [front_half * cosine - second * sine_part, second * cosine + front_half * sine_part],
        axis=-1,
    )


def norm_rows(values, gain_vec):
    as_float = values.astype(jnp.float32)
    return (
        as_float * lax.rsqrt(jnp.mean(as_float * as_float, axis=1, keepdims=True) + EPS) * gain_vec
    ).astype(jnp.bfloat16)


def attend(running, q_nope, q_rot, key_rows, value_rows, rot_keys, lat_scale):
    prior_max, denom_sum, weighted = running
    scores = (
        jnp.einsum("qhd,khd->hqk", q_nope, key_rows, preferred_element_type=jnp.float32)
        + jnp.einsum("qhr,kr->hqk", q_rot, rot_keys, preferred_element_type=jnp.float32)
    ) * lat_scale
    row_max = jnp.maximum(prior_max, jnp.max(scores, axis=2))
    rescale = jnp.exp(prior_max - row_max)
    weights = jnp.exp(scores - row_max[:, :, None])
    denom_sum = denom_sum * rescale + jnp.sum(weights, axis=2)
    weighted = weighted * rescale.T[:, :, None] + jnp.einsum(
        "hqk,khd->qhd", weights.astype(jnp.bfloat16), value_rows, preferred_element_type=jnp.float32
    )
    return (row_max, denom_sum, weighted)


def in_blocks(running, arrays, block_fn):
    key_count = arrays[0].shape[0]
    blocked = tuple(
        (member.reshape((key_count // key_span, key_span) + member.shape[1:]) for member in arrays)
    )

    def scan_step(state_now, key_block):
        return (block_fn(state_now, key_block), None)

    running, unused = lax.scan(scan_step, running, blocked)
    return running


def per_device(
    tokens,
    norm_gain,
    window_query,
    window_key,
    window_value,
    sink_logit,
    down_query,
    down_latent,
    rotary_proj,
    query_gain,
    latent_gain,
    up_query,
    up_key,
    up_value,
    window_out,
    latent_out,
):
    row_count = tokens.shape[0]
    projections = (window_query, window_key, window_value, down_query, down_latent, rotary_proj)
    start_carry = (jnp.zeros((row_count,), jnp.float32),) + tuple(
        (jnp.zeros((row_count, weight.shape[1]), jnp.float32) for weight in projections)
    )
    as_float = lax.all_gather(tokens, "tp", axis=1, tiled=True).astype(jnp.float32)
    scaled = (as_float * norm_gain[None, :]).astype(jnp.bfloat16)
    updated = [jnp.sum(as_float * as_float, axis=1)]
    for total_now, weight in zip(start_carry[1:], projections):
        updated.append(jnp.dot(scaled, weight, preferred_element_type=jnp.float32))
    folded = tuple(updated)
    row_scale = lax.rsqrt(folded[0] / D + EPS)[:, None]
    q_window, k_window, v_window, latent_q, latent_kv, rotary_rows = [
        (member * row_scale).astype(jnp.bfloat16) for member in folded[1:]
    ]
    seq_index = lax.axis_index("sp")
    positions = seq_index * row_count + jnp.arange(row_count, dtype=jnp.int32)
    heads_dev = window_query.shape[1] // HD
    kv_dev = window_key.shape[1] // HD
    group = heads_dev // kv_dev
    stacked = jnp.concatenate([k_window, v_window], axis=1)
    padded = with_halo(stacked, (("sp", 0),), WINDOW)
    span_len = QBLOCK + 2 * WINDOW
    block_count = row_count // QBLOCK
    spans = jnp.stack(
        [
            padded[block_num * QBLOCK : block_num * QBLOCK + span_len]
            for block_num in range(block_count)
        ]
    )
    key_part = spans[..., : kv_dev * HD].reshape(block_count, span_len, kv_dev, HD)
    value_part = spans[..., kv_dev * HD :].reshape(block_count, span_len, kv_dev, HD)
    queries = q_window.reshape(block_count, QBLOCK, kv_dev, group, HD)
    scores = jnp.einsum(
        "nqhgd,nkhd->nhgqk", queries, key_part, preferred_element_type=jnp.float32
    ) * HD ** (-0.5)
    distance = jnp.arange(QBLOCK)[:, None] + WINDOW - jnp.arange(span_len)[None, :]
    head_ids = lax.axis_index("tp") * heads_dev + jnp.arange(heads_dev, dtype=jnp.int32)
    slopes = jnp.exp2(-8.0 * (head_ids.astype(jnp.float32) + 1.0) / A_HEADS).reshape(kv_dev, group)
    scores = scores - slopes[None, :, :, None, None] * jnp.abs(distance).astype(jnp.float32)
    key_pos = (
        seq_index * row_count
        + (jnp.arange(block_count, dtype=jnp.int32) * QBLOCK)[:, None]
        + jnp.arange(span_len, dtype=jnp.int32)[None, :]
        - WINDOW
    )
    seq_len = row_count * lax.axis_size("sp")
    valid = (jnp.abs(distance) <= WINDOW)[None] & ((key_pos >= 0) & (key_pos < seq_len))[:, None, :]
    scores = jnp.where(valid[:, None, None], scores, -jnp.inf)
    sinks = sink_logit.reshape(kv_dev, group)[None, :, :, None, None]
    row_max = jnp.maximum(jnp.max(scores, axis=4, keepdims=True), sinks)
    weights = jnp.exp(scores - row_max)
    weights = weights / (jnp.sum(weights, axis=4, keepdims=True) + jnp.exp(sinks - row_max))
    out_window = (
        jnp.einsum(
            "nhgqk,nkhd->nqhgd",
            weights.astype(jnp.bfloat16),
            value_part,
            preferred_element_type=jnp.float32,
        )
        .astype(jnp.bfloat16)
        .reshape(row_count, heads_dev * HD)
    )
    latent_heads = up_query.shape[1] // (NOPE + ROPE)
    q_latent = jnp.dot(
        norm_rows(latent_q, query_gain), up_query, preferred_element_type=jnp.float32
    ).astype(jnp.bfloat16)
    q_latent = q_latent.reshape(row_count, latent_heads, NOPE + ROPE)
    q_nope = q_latent[..., :NOPE]
    q_rot = rotate(q_latent[..., NOPE:], positions).astype(jnp.bfloat16)
    k_rot = rotate(rotary_rows, positions).astype(jnp.bfloat16)
    normed_kv = norm_rows(latent_kv, latent_gain)
    lat_scale = (NOPE + ROPE) ** (-0.5)
    start_state = (
        jnp.full((latent_heads, row_count), -1e30, jnp.float32),
        jnp.zeros((latent_heads, row_count), jnp.float32),
        jnp.zeros((row_count, latent_heads, VD), jnp.float32),
    )
    key_rows = jnp.dot(normed_kv, up_key, preferred_element_type=jnp.float32).astype(jnp.bfloat16)
    value_rows = jnp.dot(normed_kv, up_value, preferred_element_type=jnp.float32).astype(
        jnp.bfloat16
    )
    paired = jnp.concatenate([key_rows, value_rows], axis=1)

    def split_block(running, key_block):
        pair_part, rot_part = key_block
        key_count = pair_part.shape[0]
        return attend(
            running,
            q_nope,
            q_rot,
            pair_part[:, : latent_heads * NOPE].reshape(key_count, latent_heads, NOPE),
            pair_part[:, latent_heads * NOPE :].reshape(key_count, latent_heads, VD),
            rot_part,
            lat_scale,
        )

    final_state = in_blocks(
        start_state,
        (
            lax.all_gather(paired, "sp", axis=0, tiled=True),
            lax.all_gather(k_rot, "sp", axis=0, tiled=True),
        ),
        split_block,
    )
    out_latent = (
        (final_state[2] / final_state[1].T[:, :, None])
        .astype(jnp.bfloat16)
        .reshape(row_count, latent_heads * VD)
    )
    return lax.psum_scatter(
        (
            jnp.dot(out_window, window_out, preferred_element_type=jnp.float32)
            + jnp.dot(out_latent, latent_out, preferred_element_type=jnp.float32)
        ).astype(jnp.bfloat16),
        "tp",
        scatter_dimension=0,
        tiled=True,
    )


def solution(mesh):
    placed = (
        P("sp", "tp"),
        P(),
        P(None, "tp"),
        P(None, "tp"),
        P(None, "tp"),
        P("tp"),
        P(),
        P(),
        P(),
        P(),
        P(),
        P(None, "tp"),
        P(None, "tp"),
        P(None, "tp"),
        P("tp", None),
        P("tp", None),
    )
    return jax.shard_map(
        per_device, mesh=mesh, in_specs=placed, out_specs=P(("sp", "tp"), None), check_vma=False
    )
```

profile of v0, /device:TPU:0, one launch (start us, length us, event | category | flops | bytes accessed | tf_op | source)
XLA Modules:
  0.0 329.1 jit_solution(16561795479787083009)
XLA Ops:
  7.3 32.9 %all-gather.3.cloned.1.call-done = bf16[768,2048]{1,0:T(8,128)(2,1)} async-done(((bf16[768,512]{1,0:T(8,128)(2,1)}), bf16[768,2048]{1,0:T(8,128)(2,1)}) %all-gather.3.cloned.1.call-update) | async-done | bytes 3145744 | tf_op jit(solution)/shard_map/all_gather | solution.py:108
  40.2 2.7 fusion.18
  43.0 3.5 %fusion.26 = (f32[768]{0:T(1024)S(1)}, bf16[768,512]{0,1:T(8,128)(2,1)S(1)}) fusion(f32[768]{0:T(1024)S(1)} %add_rsqrt_fusion.2, bf16[2048,512]{1,0:T(8,128)(2,1)} %param.25, bf16[768,2048]{1,0:T(8,128)(2,1)S(1)} %copy-done.6, f32[2048]{0:T(1024)S(1)} %copy-done.25), kind=kOutput, calls=%fused_computation.39 | convolution fusion | flops 1617296640 | bytes 6043648 | tf_op jit(solution)/shard_map/dot_general | solution.py:112
  54.9 4.0 %collective-permute-start = (bf16[128,256]{0,1:T(8,128)(2,1)}, bf16[128,256]{0,1:T(8,128)(2,1)}, u32[]{:S(2)}, u32[]{:S(2)}) collective-permute-start(bf16[128,256]{0,1:T(8,128)(2,1)} %get-tuple-element.122), channel_id=1, source_target_pairs={{0,4},{4,8},{8,12},{12,16},{16,20},{20,24},{24,28},{1,5},{5,9},{9,... | collective-permute-start | bytes 196616 | tf_op jit(solution)/shard_map/ppermute | solution.py:28
  62.2 34.6 %all_gather.11 = bf16[6144,32]{0,1:T(8,128)(2,1)S(1)} all-gather(bf16[768,32]{0,1:T(8,128)(2,1)S(1)} %pad_maximum_fusion.9), channel_id=1, replica_groups=mesh['sp'=8,'tp'=4] {'sp'}, dimensions={0}, use_global_device_ids=true | all-gather | bytes 442368 | tf_op jit(solution)/shard_map/all_gather | solution.py:204
  99.3 2.8 reshape.240
  102.1 4.7 %fusion.23 = (f32[768]{0:T(1024)S(1)}, bf16[768,768]{0,1:T(8,128)(2,1)S(1)}) fusion(f32[768]{0:T(1024)} %copy-done.16, bf16[2048,768]{1,0:T(8,128)(2,1)S(1)} %copy-done, bf16[768,2048]{1,0:T(8,128)(2,1)} %all-gather.3.cloned.1.call-done, f32[2048]{0:T(1024)} %param.19), kind=kOutput, calls=%fused_computation.33 | convolution fusion | flops 2423586048 | bytes 7485440 | tf_op jit(solution)/shard_map/dot_general | solution.py:112
  113.2 2.0 fusion.42
  115.7 3.6 %fusion.91 = f32[768,2048]{1,0:T(8,128)} fusion(bf16[768,256]{0,1:T(8,128)(2,1)S(1)} %bitcast.110, bf16[256,2048]{1,0:T(8,128)(2,1)S(1)} %copy-done.8), kind=kOutput, calls=%fused_computation.124 | convolution fusion | flops 805306368 | bytes 7733248 | tf_op jit(solution)/shard_map/dot_general | solution.py:215
  119.3 32.7 %all-gather.5.cloned.1.call-done = bf16[6144,512]{0,1:T(8,128)(2,1)} async-done(((bf16[768,512]{0,1:T(8,128)(2,1)}), bf16[6144,512]{0,1:T(8,128)(2,1)}) %all-gather.5.cloned.1.call-update) | async-done | bytes 6291472 | tf_op jit(solution)/shard_map/all_gather | solution.py:203
  152.0 8.7 %copy.27 = bf16[6144,512]{1,0:T(8,128)(2,1)} copy(bf16[6144,512]{0,1:T(8,128)(2,1)} %all-gather.5.cloned.1.call-done) | data formatting | bytes 12582912 | tf_op jit(solution)/shard_map/all_gather | solution.py:203
  160.7 118.2 %while.15 = (s32[]{:T(128)}, f32[4,768]{1,0:T(4,128)S(1)}, f32[4,768]{1,0:T(4,128)S(1)}, f32[768,4,64]{0,2,1:T(8,128)}, bf16[6,1024,512]{2,1,0:T(8,128)(2,1)}, /...) while((s32[]{:T(128)}, f32[4,768]{1,0:T(4,128)S(1)}, ...), condition=%wide.region_8.9_spmd.clone, body=%wide.region_5.8_spmd.clone.sunk | while | flops 1029261312 | bytes 78971056 | solution.py:81
  162.6 6.4 %fusion.129 = f32[4,1024,768]{2,1,0:T(8,128)} fusion(bf16[1024,4,64]{0,2,1:T(8,128)(2,1)S(1)} %bitcast.107, bf16[768,4,64]{0,2,1:T(8,128)(2,1)S(1)} %get-tuple-element.222), kind=kOutput, calls=%fused_computation.123.clone.1 | convolution fusion | flops 402653184 | bytes 13500416 | tf_op jit(solution)/shard_map/while/body/eval_jaxpr/qhd,khd->hqk/dot_general | solution.py:59
  169.0 6.5 %fusion.130 = (f32[4,768]{1,0:T(4,128)S(1)}, f32[4,768,1024]{1,2,0:T(8,128)S(1)}) fusion(bf16[768,4,32]{0,2,1:T(8,128)(2,1)S(1)} %get-tuple-element.224, bf16[6,1024,32]{1,2,0:T(8,128)(2,1)} %get-tuple-element.223, s32[]{:T(128)S(6)} %copy.51, f32[4,1024,768]{2,1,0:T(8,128)} %fusion.129), kind=kOutput, calls=%fused_computation.121.clone.1 | convolution fusion | flops 210760704 | bytes 25440260 | tf_op jit(solution)/shard_map/while/body/eval_jaxpr/qhr,kr->hqk/dot_general | solution.py:60
  177.1 2.3 fusion.134
  182.3 6.4 %fusion.129 = f32[4,1024,768]{2,1,0:T(8,128)} fusion(bf16[1024,4,64]{0,2,1:T(8,128)(2,1)S(1)} %bitcast.107, bf16[768,4,64]{0,2,1:T(8,128)(2,1)S(1)} %get-tuple-element.222), kind=kOutput, calls=%fused_computation.123.clone.1 | convolution fusion | flops 402653184 | bytes 13500416 | tf_op jit(solution)/shard_map/while/body/eval_jaxpr/qhd,khd->hqk/dot_general | solution.py:59
  188.7 6.5 %fusion.130 = (f32[4,768]{1,0:T(4,128)S(1)}, f32[4,768,1024]{1,2,0:T(8,128)S(1)}) fusion(bf16[768,4,32]{0,2,1:T(8,128)(2,1)S(1)} %get-tuple-element.224, bf16[6,1024,32]{1,2,0:T(8,128)(2,1)} %get-tuple-element.223, s32[]{:T(128)S(6)} %copy.51, f32[4,1024,768]{2,1,0:T(8,128)} %fusion.129), kind=kOutput, calls=%fused_computation.121.clone.1 | convolution fusion | flops 210760704 | bytes 25440260 | tf_op jit(solution)/shard_map/while/body/eval_jaxpr/qhr,kr->hqk/dot_general | solution.py:60
  196.8 2.3 fusion.134
  202.0 6.3 %fusion.129 = f32[4,1024,768]{2,1,0:T(8,128)} fusion(bf16[1024,4,64]{0,2,1:T(8,128)(2,1)S(1)} %bitcast.107, bf16[768,4,64]{0,2,1:T(8,128)(2,1)S(1)} %get-tuple-element.222), kind=kOutput, calls=%fused_computation.123.clone.1 | convolution fusion | flops 402653184 | bytes 13500416 | tf_op jit(solution)/shard_map/while/body/eval_jaxpr/qhd,khd->hqk/dot_general | solution.py:59
  208.4 6.5 %fusion.130 = (f32[4,768]{1,0:T(4,128)S(1)}, f32[4,768,1024]{1,2,0:T(8,128)S(1)}) fusion(bf16[768,4,32]{0,2,1:T(8,128)(2,1)S(1)} %get-tuple-element.224, bf16[6,1024,32]{1,2,0:T(8,128)(2,1)} %get-tuple-element.223, s32[]{:T(128)S(6)} %copy.51, f32[4,1024,768]{2,1,0:T(8,128)} %fusion.129), kind=kOutput, calls=%fused_computation.121.clone.1 | convolution fusion | flops 210760704 | bytes 25440260 | tf_op jit(solution)/shard_map/while/body/eval_jaxpr/qhr,kr->hqk/dot_general | solution.py:60
  216.5 2.3 fusion.134
  221.7 6.3 %fusion.129 = f32[4,1024,768]{2,1,0:T(8,128)} fusion(bf16[1024,4,64]{0,2,1:T(8,128)(2,1)S(1)} %bitcast.107, bf16[768,4,64]{0,2,1:T(8,128)(2,1)S(1)} %get-tuple-element.222), kind=kOutput, calls=%fused_computation.123.clone.1 | convolution fusion | flops 402653184 | bytes 13500416 | tf_op jit(solution)/shard_map/while/body/eval_jaxpr/qhd,khd->hqk/dot_general | solution.py:59
  228.1 6.4 %fusion.130 = (f32[4,768]{1,0:T(4,128)S(1)}, f32[4,768,1024]{1,2,0:T(8,128)S(1)}) fusion(bf16[768,4,32]{0,2,1:T(8,128)(2,1)S(1)} %get-tuple-element.224, bf16[6,1024,32]{1,2,0:T(8,128)(2,1)} %get-tuple-element.223, s32[]{:T(128)S(6)} %copy.51, f32[4,1024,768]{2,1,0:T(8,128)} %fusion.129), kind=kOutput, calls=%fused_computation.121.clone.1 | convolution fusion | flops 210760704 | bytes 25440260 | tf_op jit(solution)/shard_map/while/body/eval_jaxpr/qhr,kr->hqk/dot_general | solution.py:60
  236.2 2.3 fusion.134
  241.4 6.3 %fusion.129 = f32[4,1024,768]{2,1,0:T(8,128)} fusion(bf16[1024,4,64]{0,2,1:T(8,128)(2,1)S(1)} %bitcast.107, bf16[768,4,64]{0,2,1:T(8,128)(2,1)S(1)} %get-tuple-element.222), kind=kOutput, calls=%fused_computation.123.clone.1 | convolution fusion | flops 402653184 | bytes 13500416 | tf_op jit(solution)/shard_map/while/body/eval_jaxpr/qhd,khd->hqk/dot_general | solution.py:59
  247.8 6.4 %fusion.130 = (f32[4,768]{1,0:T(4,128)S(1)}, f32[4,768,1024]{1,2,0:T(8,128)S(1)}) fusion(bf16[768,4,32]{0,2,1:T(8,128)(2,1)S(1)} %get-tuple-element.224, bf16[6,1024,32]{1,2,0:T(8,128)(2,1)} %get-tuple-element.223, s32[]{:T(128)S(6)} %copy.51, f32[4,1024,768]{2,1,0:T(8,128)} %fusion.129), kind=kOutput, calls=%fused_computation.121.clone.1 | convolution fusion | flops 210760704 | bytes 25440260 | tf_op jit(solution)/shard_map/while/body/eval_jaxpr/qhr,kr->hqk/dot_general | solution.py:60
  255.9 2.3 fusion.134
  261.1 6.3 %fusion.129 = f32[4,1024,768]{2,1,0:T(8,128)} fusion(bf16[1024,4,64]{0,2,1:T(8,128)(2,1)S(1)} %bitcast.107, bf16[768,4,64]{0,2,1:T(8,128)(2,1)S(1)} %get-tuple-element.222), kind=kOutput, calls=%fused_computation.123.clone.1 | convolution fusion | flops 402653184 | bytes 13500416 | tf_op jit(solution)/shard_map/while/body/eval_jaxpr/qhd,khd->hqk/dot_general | solution.py:59
  267.5 6.4 %fusion.130 = (f32[4,768]{1,0:T(4,128)S(1)}, f32[4,768,1024]{1,2,0:T(8,128)S(1)}) fusion(bf16[768,4,32]{0,2,1:T(8,128)(2,1)S(1)} %get-tuple-element.224, bf16[6,1024,32]{1,2,0:T(8,128)(2,1)} %get-tuple-element.223, s32[]{:T(128)S(6)} %copy.51, f32[4,1024,768]{2,1,0:T(8,128)} %fusion.129), kind=kOutput, calls=%fused_computation.121.clone.1 | convolution fusion | flops 210760704 | bytes 25440260 | tf_op jit(solution)/shard_map/while/body/eval_jaxpr/qhr,kr->hqk/dot_general | solution.py:60
  275.6 2.3 fusion.134
  280.1 5.9 %add_convert_fusion = bf16[768,2048]{1,0:T(8,128)(2,1)} fusion(f32[768,2048]{1,0:T(8,128)} %fusion.91, bf16[768,256]{0,1:T(8,128)(2,1)S(1)} %bitcast.114, bf16[256,2048]{1,0:T(8,128)(2,1)} %param.33), kind=kOutput, calls=%fused_computation.25 | convolution fusion | flops 808452096 | bytes 10878976 | tf_op jit(solution)/shard_map/dot_general | solution.py:216
  286.0 36.6 %reduce-scatter.2.cloned.1.call-done = bf16[192,2048]{1,0:T(8,128)(2,1)} async-done(((bf16[768,2048]{1,0:T(8,128)(2,1)}), bf16[192,2048]{1,0:T(8,128)(2,1)}) %reduce-scatter.2.cloned.1.call-update) | async-done | bytes 786448 | tf_op jit(solution)/shard_map/reduce_scatter | solution.py:213
  (173 shorter events, 49.8 us)
Async XLA Ops:
  6.5 95.6 %copy-start = (bf16[2048,768]{1,0:T(8,128)(2,1)S(1)}, bf16[2048,768]{1,0:T(8,128)(2,1)}, u32[]{:S(2)}) copy-start(bf16[2048,768]{1,0:T(8,128)(2,1)} %param.24) | copy-start | bytes 9437188
  6.5 36.4 %copy-start.25 = (f32[2048]{0:T(1024)S(1)}, f32[2048]{0:T(1024)}, u32[]{:S(2)}) copy-start(f32[2048]{0:T(1024)} %param.19) | copy-start | bytes 24580
  6.5 33.6 %all-gather.3.cloned.1.call-start = ((), (), s32[]{:S(2)}) async-start(), calls=%async_computation.1 | async-start | bytes 3932160 | tf_op jit(solution)/shard_map/all_gather | solution.py:108
  7.3 144.7 %all-gather.5.cloned.1.call-start = ((), (), s32[]{:S(2)}) async-start(), calls=%async_computation.2 | async-start | bytes 7077888 | tf_op jit(solution)/shard_map/all_gather | solution.py:203
  40.2 2.8 copy-start.6
  43.0 3.5 %copy-start.16 = (f32[768]{0:T(1024)}, f32[768]{0:T(1024)S(1)}, u32[]{:S(2)}) copy-start(f32[768]{0:T(1024)S(1)} %add_rsqrt_fusion.2) | copy-start | bytes 9220
  43.0 3.6 %copy-start.22 = (bf16[512,256]{1,0:T(8,128)(2,1)S(1)}, bf16[512,256]{1,0:T(8,128)(2,1)}, u32[]{:S(2)}) copy-start(bf16[512,256]{1,0:T(8,128)(2,1)} %param.31) | copy-start | bytes 786436
  43.0 3.6 %copy-start.28 = (f32[512]{0:T(512)S(1)}, f32[512]{0:T(512)}, u32[]{:S(2)}) copy-start(f32[512]{0:T(512)} %param.28) | copy-start | bytes 6148
  43.0 4.1 %copy-start.23 = (bf16[512,256]{1,0:T(8,128)(2,1)S(1)}, bf16[512,256]{1,0:T(8,128)(2,1)}, u32[]{:S(2)}) copy-start(bf16[512,256]{1,0:T(8,128)(2,1)} %param.30) | copy-start | bytes 786436
  46.6 2.1 copy-start.29
  48.6 274.0 %reduce-scatter.2.cloned.1.call-start = ((), (), s32[]{:S(2)}) async-start(), calls=%async_computation.3 | async-start | bytes 3932160 | tf_op jit(solution)/shard_map/reduce_scatter | solution.py:213
  48.8 2.3 copy-start.7
  48.8 2.3 copy-start.20
  49.5 3.5 %copy-start.17 = (f32[768]{0:T(1024)S(1)}, f32[768]{0:T(1024)}, u32[]{:S(2)}) copy-start(f32[768]{0:T(1024)} %copy-done.16) | copy-start | bytes 9220
  49.5 3.5 %copy-start.21 = (bf16[2048,128]{1,0:T(8,128)(2,1)S(1)}, bf16[2048,128]{1,0:T(8,128)(2,1)}, u32[]{:S(2)}) copy-start(bf16[2048,128]{1,0:T(8,128)(2,1)} %param.21) | copy-start | bytes 1572868
  49.5 3.5 %copy-start.26 = (f32[2048]{0:T(1024)S(1)}, f32[2048]{0:T(1024)}, u32[]{:S(2)}) copy-start(f32[2048]{0:T(1024)} %param.19) | copy-start | bytes 24580
  53.0 8.2 %copy-start.9 = (bf16[768,128]{0,1:T(8,128)(2,1)}, bf16[768,128]{0,1:T(8,128)(2,1)S(1)}, u32[]{:S(2)}) copy-start(bf16[768,128]{0,1:T(8,128)(2,1)S(1)} %fusion.52) | copy-start | bytes 589828
  53.0 7.2 %copy-start.24 = (bf16[2048,32]{0,1:T(8,128)(2,1)S(1)}, bf16[2048,32]{0,1:T(8,128)(2,1)}, u32[]{:S(2)}) copy-start(bf16[2048,32]{0,1:T(8,128)(2,1)} %param.26) | copy-start | bytes 393220
  54.2 43.2 %copy-start.11 = (bf16[768,128]{0,1:T(8,128)(2,1)}, bf16[768,128]{0,1:T(8,128)(2,1)S(1)}, u32[]{:S(2)}) copy-start(bf16[768,128]{0,1:T(8,128)(2,1)S(1)} %fusion.55) | copy-start | bytes 589828
  54.3 43.2 %copy-start.18 = (bf16[2048,256]{1,0:T(8,128)(2,1)S(1)}, bf16[2048,256]{1,0:T(8,128)(2,1)}, u32[]{:S(2)}) copy-start(bf16[2048,256]{1,0:T(8,128)(2,1)} %param.20) | copy-start | bytes 3145732
  54.9 53.0 %collective-permute-start = (bf16[128,256]{0,1:T(8,128)(2,1)}, bf16[128,256]{0,1:T(8,128)(2,1)}, u32[]{:S(2)}, u32[]{:S(2)}) collective-permute-start(bf16[128,256]{0,1:T(8,128)(2,1)} %get-tuple-element.122), channel_id=1, source_target_pairs={{0,4},{4,8},{8,12},{12,16},{16,20},{20,24},{24,28},{1,5},{5,9},{9,... | collective-permute-start | bytes 196616 | tf_op jit(solution)/shard_map/ppermute | solution.py:28
  58.9 49.0 %collective-permute-start.1 = (bf16[128,256]{0,1:T(8,128)(2,1)}, bf16[128,256]{0,1:T(8,128)(2,1)}, u32[]{:S(2)}, u32[]{:S(2)}) collective-permute-start(bf16[128,256]{0,1:T(8,128)(2,1)} %get-tuple-element.123), channel_id=1, source_target_pairs={{4,0},{8,4},{12,8},{16,12},{20,16},{24,20},{28,24},{5,1},{9,5},{13... | collective-permute-start | bytes 196616 | tf_op jit(solution)/shard_map/ppermute | solution.py:29
  102.1 4.8 %copy-start.19 = (bf16[768,384]{1,0:T(8,128)(2,1)S(1)}, bf16[768,384]{1,0:T(8,128)(2,1)}, u32[]{:S(2)}) copy-start(bf16[768,384]{1,0:T(8,128)(2,1)} %param.29) | copy-start | bytes 1769476
  102.1 4.8 %copy-start.27 = (f32[768]{0:T(1024)S(1)}, f32[768]{0:T(1024)}, u32[]{:S(2)}) copy-start(f32[768]{0:T(1024)} %param.27) | copy-start | bytes 9220
  107.7 1.7 copy-start.2
  107.7 1.9 copy-start.5
  113.2 2.5 copy-start.8
  119.3 41.4 %copy-start.13 = (f32[4,768]{1,0:T(4,128)S(1)}, f32[4,768]{1,0:T(4,128)}, u32[]{:S(2)}) copy-start(f32[4,768]{1,0:T(4,128)} %custom-call.1) | copy-start | bytes 36868
  214.8 1.7 copy-start.3
  234.5 1.7 copy-start.3
  254.2 1.7 copy-start.3
  280.1 42.5 %copy-start.1 = (bf16[2048,768]{1,0:T(8,128)(2,1)S(1)}, bf16[2048,768]{1,0:T(8,128)(2,1)}, u32[]{:S(2)}) copy-start(bf16[2048,768]{1,0:T(8,128)(2,1)} %param.24) | copy-start | bytes 9437188
  (13 other events, 14.8 us)
Sparse Core Ops, SparseCore 0:
  8.9 31.2 all-gather.2
  48.7 103.2 all-gather.4
  286.1 36.4 reduce-scatter.1
where the time goes:
time: 330 us; the launch traced here: 329 us
  matrix products  120 us (36%)
  waiting for transfers between devices  103 us (31%)
  blocking collectives  34.6 us (10%)
  local copies, waits for them, and re-layouts  30.6 us (9%)
  other arithmetic  21.8 us (7%)
  between operations  13.6 us (4%)
  starting transfers between devices  5.34 us (2%)
    dot_general x6, matrix products, attend(): jnp.einsum('qhr,kr->hqk', q_rot, rot_keys, preferred_element_type=jnp.flo...  38.7 us
    dot_general x6, matrix products, attend(): jnp.einsum('qhd,khd->hqk', q_nope, key_rows, preferred_element_type=jnp.f...  38.1 us
    reduce_scatter x1, waiting for transfers between devices, per_device(): lax.psum_scatter((jnp.dot(out_window, window_out, preferred_element_type=...  36.6 us
    all_gather x1, blocking collectives, per_device(): lax.all_gather(k_rot, 'sp', axis=0, tiled=True)  34.6 us
    all_gather x1, waiting for transfers between devices, per_device(): lax.all_gather(tokens, 'tp', axis=1, tiled=True).astype(jnp.float32)  32.9 us
    all_gather x1, waiting for transfers between devices, per_device(): lax.all_gather(paired, 'sp', axis=0, tiled=True)  32.7 us
    dot_general x6, matrix products, per_device(): updated.append(jnp.dot(scaled, weight, preferred_element_type=jnp.float32))  14.1 us
    dot_general x6, matrix products, attend(): jnp.einsum('hqk,khd->qhd', weights.astype(jnp.bfloat16), value_rows, pref...  13.7 us
  transfers between devices with their start and end apart: 5, of which 3 were waited for; matrix products, arithmetic and copies ran while one was open for 9% of the time, Pallas kernels for 0%

commit v1 on v0

v1 whole, which is shorter than its diff:
```python
import functools

import jax
import jax.numpy as jnp
from jax import lax
from jax.experimental import pallas as pl
from jax.experimental.pallas import tpu as pltpu
from jax.sharding import PartitionSpec as P

A_HEADS = 16
HD = 64
NOPE = 64
ROPE = 32
VD = 64
WINDOW = 128
QBLOCK = 256
EPS = 1e-06
THETA = 10000.0
LANES = 128
LOG2E = 1.4426950408889634
VMEM_LIMIT = 60 * 1024 * 1024
BF = jnp.bfloat16
F32 = jnp.float32


def vmem():
    return pl.BlockSpec(memory_space=pltpu.VMEM)


def fdot(a, b):
    return jnp.dot(a, b, preferred_element_type=F32)


def fdot_t(a, b):
    return lax.dot_general(a, b, (((1,), (1,)), ((), ())), preferred_element_type=F32)


def normed(values, gain):
    v = values.astype(F32)
    return (v * lax.rsqrt(jnp.mean(v * v, axis=1, keepdims=True) + EPS) * gain).astype(BF)


def rotated(rope, cos, sin):
    half = ROPE // 2
    swapped = jnp.concatenate([rope[:, half:], rope[:, :half]], axis=1)
    return (rope * cos + swapped * sin).astype(BF)


def project_kernel(x, gain, wq, wk, wv, dq, dl, rp, qg, lg, uq, cs, sn,
                   qw_out, kv_out, q_out, g_out, *, block, heads, tp):
    rows = x.shape[0]
    own = rows // tp
    kvr = dl.shape[1]
    kcols = wk.shape[1]
    gain_row = gain[...]

    def scaled_rows(xs):
        xf = xs.astype(F32)
        rs = lax.rsqrt(jnp.mean(xf * xf, axis=1, keepdims=True) + EPS)
        return (xf * gain_row).astype(BF), rs

    start = pl.multiple_of(lax.axis_index("tp") * own, 16)
    mine = pl.ds(start, own)
    sc, rs = scaled_rows(x[mine, :])
    g_out[:, :kvr] = normed((fdot(sc, dl[...]) * rs).astype(BF), lg[...])
    rot = (fdot(sc, rp[...]) * rs).astype(BF).astype(F32)
    g_out[:, kvr:kvr + ROPE] = rotated(rot, cs[mine, :], sn[mine, :])
    g_out[:, kvr + ROPE:] = jnp.zeros((own, g_out.shape[1] - kvr - ROPE), BF)

    @pl.loop(0, rows // block)
    def _(i):
        at = pl.ds(pl.multiple_of(i * block, block), block)
        sc, rs = scaled_rows(x[at, :])
        qw_out[at, :] = (fdot(sc, wq[...]) * rs).astype(BF)
        kv_out[at, :kcols] = (fdot(sc, wk[...]) * rs).astype(BF)
        kv_out[at, kcols:] = (fdot(sc, wv[...]) * rs).astype(BF)
        nq = normed((fdot(sc, dq[...]) * rs).astype(BF), qg[...])
        ql = fdot(nq, uq[...]).astype(BF).astype(F32)
        cos, sin = cs[at, :], sn[at, :]
        for h in range(heads):
            base = h * (NOPE + ROPE)
            q_out[h, at, :NOPE] = ql[:, base:base + NOPE].astype(BF)
            q_out[h, at, NOPE:NOPE + ROPE] = rotated(
                ql[:, base + NOPE:base + NOPE + ROPE], cos, sin)
            q_out[h, at, NOPE + ROPE:] = jnp.zeros((block, LANES - NOPE - ROPE), BF)


def window_kernel(q, kv, before, after, sink, slope, out, pad, *, kv_dev, group, sp):
    rows = q.shape[0]
    me = lax.axis_index("sp")
    kcols = kv_dev * HD
    pad[:WINDOW, :] = before[...]
    pad[WINDOW:WINDOW + rows, :] = kv[...]
    pad[WINDOW + rows:, :] = after[...]
    span = QBLOCK + 2 * WINDOW
    dist = jnp.abs(
        lax.broadcasted_iota(jnp.int32, (QBLOCK, span), 0) + WINDOW
        - lax.broadcasted_iota(jnp.int32, (QBLOCK, span), 1))
    distf = dist.astype(F32)
    col = lax.broadcasted_iota(jnp.int32, (QBLOCK, span), 1)

    @pl.loop(0, rows // QBLOCK)
    def _(b):
        at = pl.multiple_of(b * QBLOCK, QBLOCK)
        pos = me * rows + at - WINDOW + col
        valid = (dist <= WINDOW) & (pos >= 0) & (pos < rows * sp)
        for g in range(kv_dev):
            keys = pad[pl.ds(at, span), g * HD:(g + 1) * HD]
            vals = pad[pl.ds(at, span), kcols + g * HD:kcols + (g + 1) * HD]
            for j in range(group):
                h = g * group + j
                s = fdot_t(q[pl.ds(at, QBLOCK), h * HD:(h + 1) * HD], keys) * HD ** (-0.5)
                s = jnp.where(valid, s - slope[0, h] * distf, -jnp.inf)
                snk = sink[0, h]
                m = jnp.maximum(jnp.max(s, axis=1, keepdims=True), snk)
                e = jnp.exp(s - m)
                w = e / (jnp.sum(e, axis=1, keepdims=True) + jnp.exp(snk - m))
                out[pl.ds(at, QBLOCK), h * HD:(h + 1) * HD] = fdot(w.astype(BF), vals).astype(BF)


def latent_kernel(q, g, ukv, out, ks, vs, s0, s1, *, heads, qb, kc, eb):
    rows = q.shape[1]
    total = g.shape[0]
    kvr = ukv.shape[0]
    kcols = heads * NOPE
    nq = rows // qb
    steps = heads * nq
    mult = LOG2E * (NOPE + ROPE) ** (-0.5)

    @pl.loop(0, total // eb)
    def _(c):
        at = pl.ds(pl.multiple_of(c * eb, eb), eb)
        both = fdot(g[at, :kvr], ukv[...]).astype(BF)
        tail = g[at, kvr:kvr + LANES - NOPE]
        lane = lax.broadcasted_iota(jnp.int32, (eb, LANES - VD), 1)
        one = jnp.where(lane == 0, 1.0, 0.0).astype(BF)
        for h in range(heads):
            ks[h, at, :NOPE] = both[:, h * NOPE:(h + 1) * NOPE]
            ks[h, at, NOPE:] = tail
            vs[h, at, :VD] = both[:, kcols + h * VD:kcols + (h + 1) * VD]
            vs[h, at, VD:] = one

    def q_of(i):
        return q[i // nq, pl.ds(pl.multiple_of(lax.rem(i, nq) * qb, qb), qb), :]

    def score(i, dst, c, top):
        at = slice(c * kc, (c + 1) * kc)
        s = fdot_t(q_of(i), ks[i // nq, at, :])
        dst[:, at] = s
        for j in range(kc // LANES):
            part = s[:, j * LANES:(j + 1) * LANES]
            top = part if top is None else jnp.maximum(top, part)
        return top

    def fold(i, src, c, shift, acc):
        at = slice(c * kc, (c + 1) * kc)
        p = jnp.exp2(src[:, at] * mult - shift).astype(BF)
        o = fdot(p, vs[i // nq, at, :])
        return o if acc is None else acc + o

    def finish(i, acc):
        h = i // nq
        res = (acc[:, :VD] / acc[:, VD:VD + 1]).astype(BF)
        out[h, pl.ds(pl.multiple_of(lax.rem(i, nq) * qb, qb), qb), :] = res

    def shift_of(top):
        return jnp.max(top, axis=1, keepdims=True) * mult

    chunks = total // kc
    top = None
    for c in range(chunks):
        top = score(0, s0, c, top)

    def pair(i, shift):
        for cur, nxt in ((s0, s1), (s1, s0)):
            top, acc = None, None
            following = jnp.minimum(i + 1, steps - 1)
            for c in range(chunks):
                top = score(following, nxt, c, top)
                acc = fold(i, cur, c, shift, acc)
            finish(i, acc)
            shift = shift_of(top)
            i = i + 1
        return shift

    lax.fori_loop(0, steps // 2, lambda t, s: pair(2 * t, s), shift_of(top))


def per_device(tokens, norm_gain, window_query, window_key, window_value, sink_logit, down_query,
               down_latent, rotary_proj, query_gain, latent_gain, up_query, up_key, up_value,
               window_out, latent_out):
    rows = tokens.shape[0]
    sp, tp = lax.axis_size("sp"), lax.axis_size("tp")
    heads = up_query.shape[1] // (NOPE + ROPE)
    heads_dev = window_query.shape[1] // HD
    kv_dev = window_key.shape[1] // HD
    group = heads_dev // kv_dev
    kvr = down_latent.shape[1]
    gw = kvr + LANES
    own = rows // tp
    seq = lax.axis_index("sp")
    half = ROPE // 2
    inverse = THETA ** (-jnp.arange(half, dtype=F32) / half)
    angles = (seq * rows + jnp.arange(rows, dtype=jnp.int32)).astype(F32)[:, None] * inverse[None]
    c, s = jnp.cos(angles), jnp.sin(angles)
    cs, sn = jnp.concatenate([c, c], 1), jnp.concatenate([-s, s], 1)

    x = lax.all_gather(tokens, "tp", axis=1, tiled=True)
    qw, kv, q, g = pl.pallas_call(
        functools.partial(project_kernel, block=256, heads=heads, tp=tp),
        out_shape=(
            jax.ShapeDtypeStruct((rows, heads_dev * HD), BF),
            jax.ShapeDtypeStruct((rows, 2 * kv_dev * HD), BF),
            jax.ShapeDtypeStruct((heads, rows, LANES), BF),
            jax.ShapeDtypeStruct((own, gw), BF),
        ),
        in_specs=[vmem()] * 13,
        out_specs=[vmem()] * 4,
        compiler_params=pltpu.CompilerParams(vmem_limit_bytes=VMEM_LIMIT),
        name="project",
    )(x, norm_gain[None], window_query, window_key, window_value, down_query, down_latent,
      rotary_proj, query_gain[None], latent_gain[None], up_query, cs, sn)

    g_all = lax.all_gather(g, ("sp", "tp"), axis=0, tiled=True)
    up = [(i, i + 1) for i in range(sp - 1)]
    before = lax.ppermute(kv[rows - WINDOW:], "sp", up)
    after = lax.ppermute(kv[:WINDOW], "sp", [(j, i) for i, j in up])

    ids = lax.axis_index("tp") * heads_dev + jnp.arange(heads_dev, dtype=jnp.int32)
    slopes = jnp.exp2(-8.0 * (ids.astype(F32) + 1.0) / A_HEADS)[None]
    smem = pl.BlockSpec(memory_space=pltpu.SMEM)
    out_window = pl.pallas_call(
        functools.partial(window_kernel, kv_dev=kv_dev, group=group, sp=sp),
        out_shape=jax.ShapeDtypeStruct((rows, heads_dev * HD), BF),
        in_specs=[vmem()] * 4 + [smem] * 2,
        out_specs=vmem(),
        scratch_shapes=[pltpu.VMEM((rows + 2 * WINDOW, 2 * kv_dev * HD), BF)],
        compiler_params=pltpu.CompilerParams(vmem_limit_bytes=VMEM_LIMIT),
        cost_estimate=pl.CostEstimate(flops=2 * 10**9, bytes_accessed=2**21, transcendentals=2**21),
        name="window",
    )(qw, kv, before, after, sink_logit[None], slopes)

    total = rows * sp
    ukv = jnp.concatenate([up_key, up_value], axis=1)
    out_latent = pl.pallas_call(
        functools.partial(latent_kernel, heads=heads, qb=256, kc=1024, eb=512),
        out_shape=jax.ShapeDtypeStruct((heads, rows, VD), BF),
        in_specs=[vmem()] * 3,
        out_specs=vmem(),
        scratch_shapes=[
            pltpu.VMEM((heads, total, LANES), BF),
            pltpu.VMEM((heads, total, LANES), BF),
            pltpu.VMEM((256, total), F32),
            pltpu.VMEM((256, total), F32),
        ],
        compiler_params=pltpu.CompilerParams(vmem_limit_bytes=VMEM_LIMIT),
        name="latent",
    )(q, g_all, ukv)
    out_latent = out_latent.transpose(1, 0, 2).reshape(rows, heads * VD)
    share = (fdot(out_window, window_out) + fdot(out_latent, latent_out)).astype(BF)
    return lax.psum_scatter(share, "tp", scatter_dimension=0, tiled=True)


def solution(mesh):
    placed = (
        P("sp", "tp"), P(), P(None, "tp"), P(None, "tp"), P(None, "tp"), P("tp"), P(), P(), P(),
        P(), P(), P(None, "tp"), P(None, "tp"), P(None, "tp"), P("tp", None), P("tp", None),
    )
    return jax.shard_map(
        per_device, mesh=mesh, in_specs=placed, out_specs=P(("sp", "tp"), None), check_vma=False
    )
```

time: 330 us -> 221 us (0.67)
  matrix products: 120 us -> 3.64 us
  Pallas kernels: 0 us -> 65.5 us
  blocking collectives: 34.6 us -> 0 us
  local copies, waits for them, and re-layouts: 30.6 us -> 8.06 us
  other arithmetic: 21.8 us -> 1.78 us
  waiting for transfers between devices: 103 us -> 123 us
    dot_general x31 -> x2, matrix products: 120 us -> 3.64 us  [fdot(): return jnp.dot(a, b, preferred_element_type=F32)]
    pallas_call x0 -> x3, Pallas kernels: none -> 65.5 us  [the longest x1 42.3 us: per_device(): pl.pallas_call(functools.partial(latent_kernel, heads=heads, qb=256, kc=1...]
    all_gather x1 -> x0, blocking collectives: 34.6 us -> none  [per_device(): lax.all_gather(k_rot, 'sp', axis=0, tiled=True)]
    all_gather x2, waiting for transfers between devices: 65.6 us -> 83.8 us  [the longest x1 56.3 us: per_device(): g_all = lax.all_gather(g, ('sp', 'tp'), axis=0, tiled=True)]
    reduce_sum x8 -> x0, other arithmetic: 14.3 us -> none  [the longest x6 9.99 us: attend(): denom_sum = denom_sum * rescale + jnp.sum(weights, axis=2)]
    dynamic_slice x12 -> x0, local copies, waits for them, and re-layouts: 11 us -> none  [in_blocks(): running, unused = lax.scan(scan_step, running, blocked)]
    all_gather x1 -> x0, local copies, waits for them, and re-layouts: 8.72 us -> none  [per_device(): lax.all_gather(paired, 'sp', axis=0, tiled=True)]
    while x30 -> x0, local copies, waits for them, and re-layouts: 5.64 us -> none
  transfers between devices with their start and end apart: 5 -> 5, of which waited for: 3 -> 4; matrix products, arithmetic and copies ran while one was open for 9% -> 3% of each run, Pallas kernels for 0% -> 4%
where the time goes in v1:
time: 221 us
  waiting for transfers between devices  123 us (56%)
  Pallas kernels  65.5 us (30%)
  between operations  13.2 us (6%)
  local copies, waits for them, and re-layouts  8.06 us (4%)
  starting transfers between devices  6.1 us (3%)
  matrix products  3.64 us (2%)
    all_gather x1, waiting for transfers between devices, per_device(): g_all = lax.all_gather(g, ('sp', 'tp'), axis=0, tiled=True)  56.3 us
    pallas_call x1, Pallas kernels, per_device(): pl.pallas_call(functools.partial(latent_kernel, heads=heads, qb=256, kc=1...  42.3 us
    reduce_scatter x1, waiting for transfers between devices, per_device(): return lax.psum_scatter(share, 'tp', scatter_dimension=0, tiled=True)  36.7 us
    all_gather x1, waiting for transfers between devices, per_device(): x = lax.all_gather(tokens, 'tp', axis=1, tiled=True)  27.5 us
    pallas_call x1, Pallas kernels, per_device(): pl.pallas_call(functools.partial(project_kernel, block=256, heads=heads,...  15.1 us
    pallas_call x1, Pallas kernels, per_device(): pl.pallas_call(functools.partial(window_kernel, kv_dev=kv_dev, group=grou...  8.11 us
    ppermute x1, starting transfers between devices, per_device(): before = lax.ppermute(kv[rows - WINDOW:], 'sp', up)  4.73 us
  transfers between devices with their start and end apart: 5, of which 4 were waited for; matrix products, arithmetic and copies ran while one was open for 3% of the time, Pallas kernels for 4%

profile of v1, /device:TPU:0, one launch (start us, length us, event | category | flops | bytes accessed | tf_op | source)
XLA Modules:
  0.0 221.1 jit_solution(2634813745789859734)
XLA Ops:
  6.5 0.0 copy-start
  6.5 0.0 all-gather.3.cloned.1.call-start
  6.5 0.7 all-gather.3.cloned.1.call-update
  7.3 0.0 all-gather.5.cloned.1.call-start
  7.3 1.3 broadcast_in_dim.16.qg
  8.6 0.3 fusion
  8.9 0.9 copy.21.cs
  9.8 0.9 copy.22.sn
  10.8 1.9 copy.20.rp
  12.7 27.5 %all-gather.3.cloned.1.call-done.x = bf16[768,2048]{1,0:T(8,128)(2,1)} async-done(((bf16[768,512]{1,0:T(8,128)(2,1)}), bf16[768,2048]{1,0:T(8,128)(2,1)}) %all-gather.3.cloned.1.call-update) | async-done | bytes 3145744 | tf_op jit(solution)/shard_map/all_gather | solution.py:208
  40.2 15.1 %project.1 = (bf16[768,256]{1,0:T(8,128)(2,1)}, bf16[768,256]{1,0:T(8,128)(2,1)}, bf16[4,768,128]{2,1,0:T(8,128)(2,1)}, bf16[192,640]{1,0:T(8,128)(2,1)}) custom-call(bf16[768,2048]{1,0:T(8,128)(2,1)} %all-gather.3.cloned.1.call-done.x, f32[1,2048]{1,0:T(1,128)} %bitcast.11, bf16[2048,256]{1,0:T(8,128)(2,1)} %wq.1, bf16[2048,128]{1,0:T(8,128)(2,1)} %wk.1, ...), custom_call_target="tpu_custom_call" | custom-call | tf_op jit(solution)/shard_map/project/pallas_call | solution.py:209
  55.3 0.0 all-gather.5.cloned.1.call-update
  55.3 0.0 reduce-scatter.2.cloned.1.call-start
  55.4 0.0 copy-done.3
  55.4 0.0 copy-done.4
  55.4 0.9 pad_maximum_fusion.ukv
  56.3 0.9 fusion.1
  57.2 1.3 collective-permute-start.1
  58.5 4.7 %collective-permute-start = (bf16[128,256]{1,0:T(8,128)(2,1)S(1)}, bf16[128,256]{1,0:T(8,128)(2,1)S(1)}, u32[]{:S(2)}, u32[]{:S(2)}) collective-permute-start(bf16[128,256]{1,0:T(8,128)(2,1)S(1)} %get-tuple-element.14), channel_id=1, source_target_pairs={{0,4},{4,8},{8,12},{12,16},{16,20},{20,24},{24,28},{1,5},{5,9},{9,... | collective-permute-start | bytes 196616 | tf_op jit(solution)/shard_map/ppermute | solution.py:226
  63.2 0.6 multiply_exponential_fusion.slope
  63.8 0.0 collective-permute-done.1.after
  63.8 1.5 collective-permute-done.before
  65.3 0.0 copy-done.5
  65.3 0.6 copy-done.6
  65.9 8.1 %window.1 = bf16[768,256]{1,0:T(8,128)(2,1)} custom-call(bf16[768,256]{1,0:T(8,128)(2,1)} %get-tuple-element.9.q, bf16[768,256]{1,0:T(8,128)(2,1)} %get-tuple-element.10.kv, bf16[128,256]{1,0:T(8,128)(2,1)} %copy-done.6, bf16[128,256]{1,0:T(8,128)(2,1)} %copy-done.5, f32[1,4]{1,0:T(1,128)} %bitcast.13, f32[1,4]{1,0:T(1,128)} %multiply_exponential_fusion.slope), custom_call_target="tpu_custom_call" | custom-call | flops 2000000000 | bytes 2097152 | tf_op jit(solution)/shard_map/window/pallas_call | solution.py:232
  74.0 56.3 %all-gather.5.cloned.1.call-done.g = bf16[6144,640]{1,0:T(8,128)(2,1)} async-done(((bf16[192,640]{1,0:T(8,128)(2,1)}), bf16[6144,640]{1,0:T(8,128)(2,1)}) %all-gather.5.cloned.1.call-update) | async-done | bytes 7864336 | tf_op jit(solution)/shard_map/all_gather | solution.py:224
  130.4 42.3 %latent.1 = bf16[4,768,64]{2,1,0:T(8,128)(2,1)} custom-call(bf16[4,768,128]{2,1,0:T(8,128)(2,1)} %get-tuple-element.11.q, bf16[6144,640]{1,0:T(8,128)(2,1)} %all-gather.5.cloned.1.call-done.g, bf16[512,512]{1,0:T(8,128)(2,1)} %pad_maximum_fusion.ukv), custom_call_target="tpu_custom_call" | custom-call | tf_op jit(solution)/shard_map/latent/pallas_call | solution.py:245
  172.7 1.5 copy.23
  174.2 1.0 fusion.2
  175.2 2.6 %add_convert_fusion = bf16[768,2048]{1,0:T(8,128)(2,1)} fusion(f32[768,2048]{1,0:T(8,128)S(1)} %fusion.2, bf16[768,256]{1,0:T(8,128)(2,1)S(1)} %copy-done.2, bf16[256,2048]{1,0:T(8,128)(2,1)S(1)} %copy-done.1), kind=kOutput, calls=%fused_computation | convolution fusion | flops 808452096 | bytes 10878976 | tf_op jit(solution)/shard_map/dot_general | solution.py:31
  177.8 0.0 reduce-scatter.2.cloned.1.call-update
  177.9 36.7 %reduce-scatter.2.cloned.1.call-done = bf16[192,2048]{1,0:T(8,128)(2,1)} async-done(((bf16[768,2048]{1,0:T(8,128)(2,1)}), bf16[192,2048]{1,0:T(8,128)(2,1)}) %reduce-scatter.2.cloned.1.call-update) | async-done | bytes 786448 | tf_op jit(solution)/shard_map/reduce_scatter | solution.py:261
  (12 shorter events, 0.0 us)
Async XLA Ops:
  6.5 167.6 %copy-start = (bf16[256,2048]{1,0:T(8,128)(2,1)S(1)}, bf16[256,2048]{1,0:T(8,128)(2,1)}, u32[]{:S(2)}) copy-start(bf16[256,2048]{1,0:T(8,128)(2,1)} %param.31) | copy-start | bytes 3145732
  6.5 33.6 %all-gather.3.cloned.1.call-start = ((), (), s32[]{:S(2)}) async-start(), calls=%async_computation.1 | async-start | bytes 3932160 | tf_op jit(solution)/shard_map/all_gather | solution.py:208
  7.3 123.1 %all-gather.5.cloned.1.call-start = ((), (), s32[]{:S(2)}) async-start(), calls=%async_computation.2 | async-start | bytes 8110080 | tf_op jit(solution)/shard_map/all_gather | solution.py:224
  40.2 15.2 %copy-start.3 = (bf16[512,256]{1,0:T(8,128)(2,1)S(1)}, bf16[512,256]{1,0:T(8,128)(2,1)}, u32[]{:S(2)}) copy-start(bf16[512,256]{1,0:T(8,128)(2,1)} %param.29) | copy-start | bytes 786436
  40.2 15.2 %copy-start.4 = (bf16[512,256]{1,0:T(8,128)(2,1)S(1)}, bf16[512,256]{1,0:T(8,128)(2,1)}, u32[]{:S(2)}) copy-start(bf16[512,256]{1,0:T(8,128)(2,1)} %param.28) | copy-start | bytes 786436
  55.3 159.2 %reduce-scatter.2.cloned.1.call-start = ((), (), s32[]{:S(2)}) async-start(), calls=%async_computation.3 | async-start | bytes 3932160 | tf_op jit(solution)/shard_map/reduce_scatter | solution.py:261
  57.2 6.6 %collective-permute-start.1 = (bf16[128,256]{1,0:T(8,128)(2,1)S(1)}, bf16[128,256]{1,0:T(8,128)(2,1)S(1)}, u32[]{:S(2)}, u32[]{:S(2)}) collective-permute-start(bf16[128,256]{1,0:T(8,128)(2,1)S(1)} %get-tuple-element.13), channel_id=1, source_target_pairs={{4,0},{8,4},{12,8},{16,12},{20,16},{24,20},{28,24},{5,1},{9,5},{13... | collective-permute-start | bytes 196616 | tf_op jit(solution)/shard_map/ppermute | solution.py:227
  58.5 6.8 %collective-permute-start = (bf16[128,256]{1,0:T(8,128)(2,1)S(1)}, bf16[128,256]{1,0:T(8,128)(2,1)S(1)}, u32[]{:S(2)}, u32[]{:S(2)}) collective-permute-start(bf16[128,256]{1,0:T(8,128)(2,1)S(1)} %get-tuple-element.14), channel_id=1, source_target_pairs={{0,4},{4,8},{8,12},{12,16},{16,20},{20,24},{24,28},{1,5},{5,9},{9,... | collective-permute-start | bytes 196616 | tf_op jit(solution)/shard_map/ppermute | solution.py:226
  63.8 1.5 copy-start.5
  65.3 0.6 copy-start.6
  172.7 2.5 %copy-start.1 = (bf16[256,2048]{1,0:T(8,128)(2,1)S(1)}, bf16[256,2048]{1,0:T(8,128)(2,1)}, u32[]{:S(2)}) copy-start(bf16[256,2048]{1,0:T(8,128)(2,1)} %param.30) | copy-start | bytes 3145732
  172.7 2.5 %copy-start.2 = (bf16[768,256]{1,0:T(8,128)(2,1)S(1)}, bf16[768,256]{1,0:T(8,128)(2,1)}, u32[]{:S(2)}) copy-start(bf16[768,256]{1,0:T(8,128)(2,1)} %window.1) | copy-start | bytes 1179652
Sparse Core Ops, SparseCore 0:
  8.9 31.2 all-gather.2
  55.4 74.8 all-gather.4
  178.0 36.5 reduce-scatter.1

commit v2 on v1

--- a/solution.py
+++ b/solution.py
@@ -46,31 +46,35 @@
     return (rope * cos + swapped * sin).astype(BF)
 
 
-def project_kernel(x, gain, wq, wk, wv, dq, dl, rp, qg, lg, uq, cs, sn,
-                   qw_out, kv_out, q_out, g_out, *, block, heads, tp):
+def scaled_rows(xs, gain_row):
+    xf = xs.astype(F32)
+    rs = lax.rsqrt(jnp.mean(xf * xf, axis=1, keepdims=True) + EPS)
+    return (xf * gain_row).astype(BF), rs
+
+
+def compress_kernel(x, gain, dl, rp, lg, cs, sn, g0_out, g1_out):
+    kvr = dl.shape[1]
+    half = g0_out.shape[0]
+    sc, rs = scaled_rows(x[...], gain[...])
+    nkv = normed((fdot(sc, dl[...]) * rs).astype(BF), lg[...])
+    rot = (fdot(sc, rp[...]) * rs).astype(BF).astype(F32)
+    rot = rotated(rot, cs[...], sn[...])
+    for k, ref in enumerate((g0_out, g1_out)):
+        at = slice(k * half, (k + 1) * half)
+        ref[:, :kvr] = nkv[at, :]
+        ref[:, kvr:kvr + ROPE] = rot[at, :]
+        ref[:, kvr + ROPE:] = jnp.zeros((half, ref.shape[1] - kvr - ROPE), BF)
+
+
+def project_kernel(x, gain, wq, wk, wv, dq, qg, uq, cs, sn, qw_out, kv_out, q_out, *, block, heads):
     rows = x.shape[0]
-    own = rows // tp
-    kvr = dl.shape[1]
     kcols = wk.shape[1]
     gain_row = gain[...]
-
-    def scaled_rows(xs):
-        xf = xs.astype(F32)
-        rs = lax.rsqrt(jnp.mean(xf * xf, axis=1, keepdims=True) + EPS)
-        return (xf * gain_row).astype(BF), rs
-
-    start = pl.multiple_of(lax.axis_index("tp") * own, 16)
-    mine = pl.ds(start, own)
-    sc, rs = scaled_rows(x[mine, :])
-    g_out[:, :kvr] = normed((fdot(sc, dl[...]) * rs).astype(BF), lg[...])
-    rot = (fdot(sc, rp[...]) * rs).astype(BF).astype(F32)
-    g_out[:, kvr:kvr + ROPE] = rotated(rot, cs[mine, :], sn[mine, :])
-    g_out[:, kvr + ROPE:] = jnp.zeros((own, g_out.shape[1] - kvr - ROPE), BF)
 
     @pl.loop(0, rows // block)
     def _(i):
         at = pl.ds(pl.multiple_of(i * block, block), block)
-        sc, rs = scaled_rows(x[at, :])
+        sc, rs = scaled_rows(x[at, :], gain_row)
         qw_out[at, :] = (fdot(sc, wq[...]) * rs).astype(BF)
         kv_out[at, :kcols] = (fdot(sc, wk[...]) * rs).astype(BF)
         kv_out[at, kcols:] = (fdot(sc, wv[...]) * rs).astype(BF)
@@ -118,7 +122,11 @@
                 out[pl.ds(at, QBLOCK), h * HD:(h + 1) * HD] = fdot(w.astype(BF), vals).astype(BF)
 
 
-def latent_kernel(q, g, ukv, out, ks, vs, s0, s1, *, heads, qb, kc, eb):
+def latent_kernel(*refs, heads, qb, kc, eb, last):
+    if last:
+        q, g, ukv, earlier, out, ks, vs, s0, s1 = refs
+    else:
+        q, g, ukv, out, ks, vs, s0, s1 = refs
     rows = q.shape[1]
     total = g.shape[0]
     kvr = ukv.shape[0]
@@ -158,10 +166,18 @@
         o = fdot(p, vs[i // nq, at, :])
         return o if acc is None else acc + o
 
-    def finish(i, acc):
+    def finish(i, acc, shift):
         h = i // nq
-        res = (acc[:, :VD] / acc[:, VD:VD + 1]).astype(BF)
-        out[h, pl.ds(pl.multiple_of(lax.rem(i, nq) * qb, qb), qb), :] = res
+        at = pl.ds(pl.multiple_of(lax.rem(i, nq) * qb, qb), qb)
+        if last:
+            was = earlier[h, at, :]
+            was_shift = was[:, VD + 1:VD + 2]
+            top = jnp.maximum(shift, was_shift)
+            acc = acc * jnp.exp2(shift - top) + was * jnp.exp2(was_shift - top)
+            out[h, at, :] = (acc[:, :VD] / acc[:, VD:VD + 1]).astype(BF)
+        else:
+            lane = lax.broadcasted_iota(jnp.int32, acc.shape, 1)
+            out[h, at, :] = jnp.where(lane == VD + 1, shift, acc)
 
     def shift_of(top):
         return jnp.max(top, axis=1, keepdims=True) * mult
@@ -178,12 +194,64 @@
             for c in range(chunks):
                 top = score(following, nxt, c, top)
                 acc = fold(i, cur, c, shift, acc)
-            finish(i, acc)
+            finish(i, acc, shift)
             shift = shift_of(top)
             i = i + 1
         return shift
 
     lax.fori_loop(0, steps // 2, lambda t, s: pair(2 * t, s), shift_of(top))
+
+
+def mix_kernel(ow, ol, wa, wb, out, to_pair, from_pair, to_far, from_far,
+               pair_send, pair_recv, far_send, far_recv, *, chips, own):
+    me = lax.axis_index("tp")
+    chip, core = me // 2, lax.rem(me, 2)
+    pair = chip * 2 + 1 - core
+    mesh = pl.DeviceIdType.MESH
+
+    def chip_at(step):
+        return lax.rem(chip + step, chips)
+
+    def share(dest):
+        at = pl.ds(pl.multiple_of(dest * own, 16), own)
+        return (fdot(ow[at, :], wa[...]) + fdot(ol[at, :], wb[...])).astype(BF)
+
+    barrier = pltpu.get_barrier_semaphore()
+    pl.semaphore_signal(barrier, inc=1, device_id={"tp": pair}, device_id_type=mesh)
+    for step in range(1, chips):
+        pl.semaphore_signal(barrier, inc=1, device_id={"tp": chip_at(step) * 2 + core},
+                            device_id_type=mesh)
+    pl.semaphore_wait(barrier, chips)
+
+    order = list(range(1, chips)) + [0]
+    copies = []
+    for step in order:
+        to_pair[step] = share(chip_at(step) * 2 + 1 - core)
+        copy = pltpu.make_async_remote_copy(
+            to_pair.at[step], from_pair.at[step], pair_send.at[step], pair_recv.at[step],
+            device_id={"tp": pair}, device_id_type=mesh)
+        copy.start()
+        copies.append(copy)
+    far = []
+    for k, step in enumerate(order[:-1]):
+        mine = share(chip_at(step) * 2 + core).astype(F32)
+        copies[k].wait_recv()
+        to_far[step - 1] = (mine + from_pair[step].astype(F32)).astype(BF)
+        copy = pltpu.make_async_remote_copy(
+            to_far.at[step - 1], from_far.at[step - 1], far_send.at[step - 1],
+            far_recv.at[step - 1],
+            device_id={"tp": chip_at(step) * 2 + core}, device_id_type=mesh)
+        copy.start()
+        far.append(copy)
+    total = share(me).astype(F32)
+    copies[-1].wait_recv()
+    total = total + from_pair[0].astype(F32)
+    for k, copy in enumerate(far):
+        copy.wait_recv()
+        total = total + from_far[k].astype(F32)
+    out[...] = total.astype(BF)
+    for copy in copies + far:
+        copy.wait_send()
 
 
 def per_device(tokens, norm_gain, window_query, window_key, window_value, sink_logit, down_query,
@@ -206,22 +274,35 @@
     cs, sn = jnp.concatenate([c, c], 1), jnp.concatenate([-s, s], 1)
 
     x = lax.all_gather(tokens, "tp", axis=1, tiled=True)
-    qw, kv, q, g = pl.pallas_call(
-        functools.partial(project_kernel, block=256, heads=heads, tp=tp),
+    params = pltpu.CompilerParams(vmem_limit_bytes=VMEM_LIMIT)
+    first = lax.axis_index("tp") * own
+    take = lambda arr: lax.dynamic_slice_in_dim(arr, first, own, 0)
+    g0, g1 = pl.pallas_call(
+        compress_kernel,
+        out_shape=(jax.ShapeDtypeStruct((own // 2, gw), BF),) * 2,
+        in_specs=[vmem()] * 7,
+        out_specs=[vmem()] * 2,
+        compiler_params=params,
+        cost_estimate=pl.CostEstimate(flops=10**9, bytes_accessed=2**22, transcendentals=0),
+        name="compress",
+    )(take(x), norm_gain[None], down_latent, rotary_proj, latent_gain[None], take(cs), take(sn))
+    parts = [lax.all_gather(part, ("sp", "tp"), axis=0, tiled=True) for part in (g0, g1)]
+
+    qw, kv, q = pl.pallas_call(
+        functools.partial(project_kernel, block=256, heads=heads),
         out_shape=(
             jax.ShapeDtypeStruct((rows, heads_dev * HD), BF),
             jax.ShapeDtypeStruct((rows, 2 * kv_dev * HD), BF),
             jax.ShapeDtypeStruct((heads, rows, LANES), BF),
-            jax.ShapeDtypeStruct((own, gw), BF),
         ),
-        in_specs=[vmem()] * 13,
-        out_specs=[vmem()] * 4,
-        compiler_params=pltpu.CompilerParams(vmem_limit_bytes=VMEM_LIMIT),
+        in_specs=[vmem()] * 10,
+        out_specs=[vmem()] * 3,
+        compiler_params=params,
+        cost_estimate=pl.CostEstimate(flops=10**10, bytes_accessed=2**23, transcendentals=0),
         name="project",
-    )(x, norm_gain[None], window_query, window_key, window_value, down_query, down_latent,
-      rotary_proj, query_gain[None], latent_gain[None], up_query, cs, sn)
-
-    g_all = lax.all_gather(g, ("sp", "tp"), axis=0, tiled=True)
+    )(x, norm_gain[None], window_query, window_key, window_value, down_query,
+      query_gain[None], up_query, cs, sn)
+
     up = [(i, i + 1) for i in range(sp - 1)]
     before = lax.ppermute(kv[rows - WINDOW:], "sp", up)
     after = lax.ppermute(kv[:WINDOW], "sp", [(j, i) for i, j in up])
@@ -240,25 +321,41 @@
         name="window",
     )(qw, kv, before, after, sink_logit[None], slopes)
 
-    total = rows * sp
+    total = rows * sp // 2
     ukv = jnp.concatenate([up_key, up_value], axis=1)
-    out_latent = pl.pallas_call(
-        functools.partial(latent_kernel, heads=heads, qb=256, kc=1024, eb=512),
-        out_shape=jax.ShapeDtypeStruct((heads, rows, VD), BF),
-        in_specs=[vmem()] * 3,
+    state = ()
+    for part, last in zip(parts, (False, True)):
+        state = (pl.pallas_call(
+            functools.partial(latent_kernel, heads=heads, qb=256, kc=1024, eb=512, last=last),
+            out_shape=jax.ShapeDtypeStruct((heads, rows, VD if last else LANES), BF if last else F32),
+            in_specs=[vmem()] * (3 + len(state)),
+            out_specs=vmem(),
+            scratch_shapes=[
+                pltpu.VMEM((heads, total, LANES), BF),
+                pltpu.VMEM((heads, total, LANES), BF),
+                pltpu.VMEM((256, total), F32),
+                pltpu.VMEM((256, total), F32),
+            ],
+            compiler_params=params,
+            cost_estimate=pl.CostEstimate(
+                flops=2 * 10**10, bytes_accessed=2**23, transcendentals=2**23),
+            name="latent_last" if last else "latent_first",
+        )(q, part, ukv, *state),)
+    out_latent = state[0].transpose(1, 0, 2).reshape(rows, heads * VD)
+    chips = tp // 2
+    width = window_out.shape[1]
+    return pl.pallas_call(
+        functools.partial(mix_kernel, chips=chips, own=own),
+        out_shape=jax.ShapeDtypeStruct((own, width), BF),
+        in_specs=[vmem()] * 4,
         out_specs=vmem(),
-        scratch_shapes=[
-            pltpu.VMEM((heads, total, LANES), BF),
-            pltpu.VMEM((heads, total, LANES), BF),
-            pltpu.VMEM((256, total), F32),
-            pltpu.VMEM((256, total), F32),
-        ],
-        compiler_params=pltpu.CompilerParams(vmem_limit_bytes=VMEM_LIMIT),
-        name="latent",
-    )(q, g_all, ukv)
-    out_latent = out_latent.transpose(1, 0, 2).reshape(rows, heads * VD)
-    share = (fdot(out_window, window_out) + fdot(out_latent, latent_out)).astype(BF)
-    return lax.psum_scatter(share, "tp", scatter_dimension=0, tiled=True)
+        scratch_shapes=[pltpu.VMEM((chips, own, width), BF)] * 2
+        + [pltpu.VMEM((max(chips - 1, 1), own, width), BF)] * 2
+        + [pltpu.SemaphoreType.DMA((chips,))] * 4,
+        compiler_params=pltpu.CompilerParams(
+            vmem_limit_bytes=VMEM_LIMIT, collective_id=1, has_side_effects=True),
+        name="mix",
+    )(out_window, out_latent, window_out, latent_out)
 
 
 def solution(mesh):

time: 221 us -> 229 us (1.036)
  Pallas kernels: 65.5 us -> 94.6 us
  waiting for transfers between devices: 123 us -> 103 us
  local copies, waits for them, and re-layouts: 8.06 us -> 12.3 us
  matrix products: 3.64 us -> 0 us
    reduce_scatter x1 -> x0, waiting for transfers between devices: 36.7 us -> none  [per_device(): return lax.psum_scatter(share, 'tp', scatter_dimension=0, tiled=True)]
    pallas_call x1 -> x3, Pallas kernels: 15.1 us -> 43 us  [the longest x1 25.8 us: per_device(): pl.pallas_call(functools.partial(mix_kernel, chips=chips, own=own), out_s...]
    all_gather x1 -> x2, waiting for transfers between devices: 56.3 us -> 68.3 us  [per_device(): lax.all_gather(part, ('sp', 'tp'), axis=0, tiled=True)]
    ppermute x1, waiting for transfers between devices: 0.01 us -> 4.07 us  [per_device(): after = lax.ppermute(kv[:WINDOW], 'sp', [(j, i) for i, j in up])]
    dot_general x2 -> x0, matrix products: 3.64 us -> none  [fdot(): return jnp.dot(a, b, preferred_element_type=F32)]
    dynamic_slice x0 -> x3, local copies, waits for them, and re-layouts: none -> 3.36 us  [per_device(): take = lambda arr: lax.dynamic_slice_in_dim(arr, first, own, 0)]
    unnamed x15 -> x19, local copies, waits for them, and re-layouts: 2.55 us -> 4.82 us
    pallas_call x1 -> x2, Pallas kernels: 42.3 us -> 43.4 us  [per_device(): pl.pallas_call(functools.partial(latent_kernel, heads=heads, qb=256, kc=1...]
  transfers between devices with their start and end apart: 5 -> 5, of which waited for: 4 -> 4; matrix products, arithmetic and copies ran while one was open for 3% -> 3% of each run, Pallas kernels for 4% -> 19%
where the time goes in v2:
time: 229 us
  waiting for transfers between devices  103 us (45%)
  Pallas kernels  94.6 us (41%)
  between operations  13.3 us (6%)
  local copies, waits for them, and re-layouts  12.3 us (5%)
  starting transfers between devices  4.92 us (2%)
    all_gather x2, waiting for transfers between devices, per_device(): lax.all_gather(part, ('sp', 'tp'), axis=0, tiled=True)  68.3 us
    pallas_call x2, Pallas kernels, per_device(): pl.pallas_call(functools.partial(latent_kernel, heads=heads, qb=256, kc=1...  43.4 us
    all_gather x1, waiting for transfers between devices, per_device(): x = lax.all_gather(tokens, 'tp', axis=1, tiled=True)  28.8 us
    pallas_call x1, Pallas kernels, per_device(): pl.pallas_call(functools.partial(mix_kernel, chips=chips, own=own), out_s...  25.8 us
    pallas_call x1, Pallas kernels, per_device(): pl.pallas_call(functools.partial(project_kernel, block=256, heads=heads),...  13.6 us
    pallas_call x1, Pallas kernels, per_device(): pl.pallas_call(functools.partial(window_kernel, kv_dev=kv_dev, group=grou...  8.13 us
    unnamed x19, local copies, waits for them, and re-layouts  4.82 us
  transfers between devices with their start and end apart: 5, of which 4 were waited for; matrix products, arithmetic and copies ran while one was open for 3% of the time, Pallas kernels for 19%

profile of v2, /device:TPU:0, one launch (start us, length us, event | category | flops | bytes accessed | tf_op | source)
XLA Modules:
  0.0 228.5 jit_solution(7038336855778075562)
XLA Ops:
  6.5 0.7 all-gather.4.cloned.1.call-update
  7.3 0.0 all-gather.8.cloned.1.call-start
  7.3 0.3 fusion
  7.6 0.2 copy.23.sn
  7.8 0.2 copy.22.cs
  8.0 0.0 copy-start.5
  8.0 2.1 copy.26.rp
  10.1 0.6 constant_dynamic-slice_fusion.sn
  10.7 0.6 constant_dynamic-slice_fusion.1.cs
  11.3 28.8 %all-gather.4.cloned.1.call-done.x = bf16[768,2048]{1,0:T(8,128)(2,1)} async-done(((bf16[768,512]{1,0:T(8,128)(2,1)}), bf16[768,2048]{1,0:T(8,128)(2,1)}) %all-gather.4.cloned.1.call-update) | async-done | bytes 3145744 | tf_op jit(solution)/shard_map/all_gather | solution.py:276
  40.2 2.1 constant_dynamic-slice_fusion.2.x
  42.2 3.6 %compress.1 = (bf16[96,640]{1,0:T(8,128)(2,1)}, bf16[96,640]{1,0:T(8,128)(2,1)}) custom-call(bf16[192,2048]{1,0:T(8,128)(2,1)} %constant_dynamic-slice_fusion.2.x, f32[1,2048]{1,0:T(1,128)} %bitcast.7, bf16[2048,512]{1,0:T(8,128)(2,1)} %dl.1, bf16[2048,32]{1,0:T(8,128)(2,1)} %copy.26.rp, f32[1,512]{1,0:T(1,128)} %bitcast.9, ...), custom_call_target="tpu_custom_call" | custom-call | flops 1000000000 | bytes 4194304 | tf_op jit(solution)/shard_map/compress/pallas_call | solution.py:280
  45.9 0.0 all-gather.8.cloned.1.call-update
  45.9 0.0 all-gather.6.cloned.1.call-start
  45.9 0.7 all-gather.6.cloned.1.call-update
  46.6 0.6 broadcast_in_dim.17.qg
  47.3 13.6 %project.1 = (bf16[768,256]{1,0:T(8,128)(2,1)}, bf16[768,256]{1,0:T(8,128)(2,1)}, bf16[4,768,128]{2,1,0:T(8,128)(2,1)}) custom-call(bf16[768,2048]{1,0:T(8,128)(2,1)} %all-gather.4.cloned.1.call-done.x, f32[1,2048]{1,0:T(1,128)} %bitcast.8, bf16[2048,256]{1,0:T(8,128)(2,1)} %wq.1, bf16[2048,128]{1,0:T(8,128)(2,1)} %wk.1, bf16[2048,128]{1,0:T(8,128)(2,1)} %wv.1, ...), custom_call_target="tpu_custom_call" | custom-call | flops 10000000000 | bytes 8388608 | tf_op jit(solution)/shard_map/project/pallas_call | solution.py:291
  60.9 0.9 fusion.1
  61.8 3.4 %collective-permute-start = (bf16[128,256]{1,0:T(8,128)(2,1)S(1)}, bf16[128,256]{1,0:T(8,128)(2,1)S(1)}, u32[]{:S(2)}, u32[]{:S(2)}) collective-permute-start(bf16[128,256]{1,0:T(8,128)(2,1)S(1)} %get-tuple-element.16), channel_id=1, source_target_pairs={{0,4},{4,8},{8,12},{12,16},{16,20},{20,24},{24,28},{1,5},{5,9},{9,... | collective-permute-start | bytes 196616 | tf_op jit(solution)/shard_map/ppermute | solution.py:307
  65.2 1.5 collective-permute-start.1
  66.7 0.6 multiply_exponential_fusion.slope
  67.3 4.1 %collective-permute-done.1.after = bf16[128,256]{1,0:T(8,128)(2,1)S(1)} collective-permute-done((bf16[128,256]{1,0:T(8,128)(2,1)S(1)}, bf16[128,256]{1,0:T(8,128)(2,1)S(1)}, u32[]{:S(2)}, u32[]{:S(2)}) %collective-permute-start.1) | collective-permute-done | bytes 65568 | tf_op jit(solution)/shard_map/ppermute | solution.py:308
  71.3 0.6 copy-done.7
  71.9 8.1 %window.1.ow = bf16[768,256]{1,0:T(8,128)(2,1)} custom-call(bf16[768,256]{1,0:T(8,128)(2,1)} %get-tuple-element.10.q, bf16[768,256]{1,0:T(8,128)(2,1)} %get-tuple-element.11.kv, bf16[128,256]{1,0:T(8,128)(2,1)} %copy-done.6, bf16[128,256]{1,0:T(8,128)(2,1)} %copy-done.7, f32[1,4]{1,0:T(1,128)} %bitcast.10, f32[1,4]{1,0:T(1,128)} %multiply_exponential_fusion.slope), custom_call_target="tpu_custom_call" | custom-call | flops 2000000000 | bytes 2097152 | tf_op jit(solution)/shard_map/window/pallas_call | solution.py:313
  80.1 26.9 %all-gather.8.cloned.1.call-done.refs_1_ = bf16[3072,640]{1,0:T(8,128)(2,1)} async-done(((bf16[96,640]{1,0:T(8,128)(2,1)}), bf16[3072,640]{1,0:T(8,128)(2,1)}) %all-gather.8.cloned.1.call-update) | async-done | bytes 3932176 | tf_op jit(solution)/shard_map/all_gather | solution.py:289
  106.9 21.2 %latent_first.1.refs_3_ = f32[4,768,128]{2,1,0:T(8,128)} custom-call(bf16[4,768,128]{2,1,0:T(8,128)(2,1)} %get-tuple-element.12.refs_0_, bf16[3072,640]{1,0:T(8,128)(2,1)} %all-gather.8.cloned.1.call-done.refs_1_, bf16[512,512]{1,0:T(8,128)(2,1)} %copy-done.4), custom_call_target="tpu_custom_call" | custom-call | flops 20000000000 | bytes 8388608 | tf_op jit(solution)/shard_map/latent_first/pallas_call | solution.py:328
  128.2 41.5 %all-gather.6.cloned.1.call-done.refs_1_ = bf16[3072,640]{1,0:T(8,128)(2,1)} async-done(((bf16[96,640]{1,0:T(8,128)(2,1)}), bf16[3072,640]{1,0:T(8,128)(2,1)}) %all-gather.6.cloned.1.call-update) | async-done | bytes 3932176 | tf_op jit(solution)/shard_map/all_gather | solution.py:289
  169.6 22.2 %latent_last.1 = bf16[4,768,64]{2,1,0:T(8,128)(2,1)} custom-call(bf16[4,768,128]{2,1,0:T(8,128)(2,1)} %get-tuple-element.12.refs_0_, bf16[3072,640]{1,0:T(8,128)(2,1)} %all-gather.6.cloned.1.call-done.refs_1_, bf16[512,512]{1,0:T(8,128)(2,1)} %copy-done.4, f32[4,768,128]{2,1,0:T(8,128)} %latent_first.1.refs_3_), custom_call_target="tpu_custom_call" | custom-call | flops 20000000000 | bytes 8388608 | tf_op jit(solution)/shard_map/latent_last/pallas_call | solution.py:328
  191.8 1.4 copy.27
  193.2 0.9 copy.28.ol
  194.1 25.8 %mix.1 = bf16[192,2048]{1,0:T(8,128)(2,1)} custom-call(bf16[768,256]{1,0:T(8,128)(2,1)} %window.1.ow, bf16[768,256]{1,0:T(8,128)(2,1)} %copy.28.ol, bf16[256,2048]{1,0:T(8,128)(2,1)} %wa.1, bf16[256,2048]{1,0:T(8,128)(2,1)} %wb.1), custom_call_target="tpu_custom_call" | custom-call | tf_op jit(solution)/shard_map/mix/pallas_call | solution.py:347
  219.9 2.1 copy.31
  (21 shorter events, 0.1 us)
Async XLA Ops:
  6.5 33.6 %all-gather.4.cloned.1.call-start = ((), (), s32[]{:S(2)}) async-start(), calls=%async_computation | async-start | bytes 3932160 | tf_op jit(solution)/shard_map/all_gather | solution.py:276
  7.3 99.7 %all-gather.8.cloned.1.call-start = ((), (), s32[]{:S(2)}) async-start(), calls=%async_computation.2 | async-start | bytes 4055040 | tf_op jit(solution)/shard_map/all_gather | solution.py:289
  7.8 38.1 %copy-start = (f32[768,32]{1,0:T(8,128)}, f32[768,32]{1,0:T(8,128)S(1)}, u32[]{:S(2)}) copy-start(f32[768,32]{1,0:T(8,128)S(1)} %copy.23.sn) | copy-start | bytes 294916
  8.0 37.9 %copy-start.1 = (f32[768,32]{1,0:T(8,128)}, f32[768,32]{1,0:T(8,128)S(1)}, u32[]{:S(2)}) copy-start(f32[768,32]{1,0:T(8,128)S(1)} %copy.22.cs) | copy-start | bytes 294916
  8.0 38.7 %copy-start.5 = (f32[768]{0:T(1024)S(1)}, f32[768]{0:T(1024)}, u32[]{:S(2)}) copy-start(f32[768]{0:T(1024)} %param.25) | copy-start | bytes 9220
  8.0 39.2 %copy-start.2 = (bf16[512,256]{1,0:T(8,128)(2,1)S(1)}, bf16[512,256]{1,0:T(8,128)(2,1)}, u32[]{:S(2)}) copy-start(bf16[512,256]{1,0:T(8,128)(2,1)} %param.28) | copy-start | bytes 786436
  10.7 36.5 %copy-start.3 = (bf16[512,256]{1,0:T(8,128)(2,1)S(1)}, bf16[512,256]{1,0:T(8,128)(2,1)}, u32[]{:S(2)}) copy-start(bf16[512,256]{1,0:T(8,128)(2,1)} %param.29) | copy-start | bytes 786436
  45.9 123.7 %all-gather.6.cloned.1.call-start = ((), (), s32[]{:S(2)}) async-start(), calls=%async_computation.1 | async-start | bytes 4055040 | tf_op jit(solution)/shard_map/all_gather | solution.py:289
  47.3 13.6 %copy-start.4 = (bf16[512,512]{1,0:T(8,128)(2,1)}, bf16[512,512]{1,0:T(8,128)(2,1)S(1)}, u32[]{:S(2)}) copy-start(bf16[512,512]{1,0:T(8,128)(2,1)S(1)} %constant_dynamic-update-slice_fusion.refs_2_) | copy-start | bytes 1572868
  61.8 5.5 %collective-permute-start = (bf16[128,256]{1,0:T(8,128)(2,1)S(1)}, bf16[128,256]{1,0:T(8,128)(2,1)S(1)}, u32[]{:S(2)}, u32[]{:S(2)}) collective-permute-start(bf16[128,256]{1,0:T(8,128)(2,1)S(1)} %get-tuple-element.16), channel_id=1, source_target_pairs={{0,4},{4,8},{8,12},{12,16},{16,20},{20,24},{24,28},{1,5},{5,9},{9,... | collective-permute-start | bytes 196616 | tf_op jit(solution)/shard_map/ppermute | solution.py:307
  65.2 6.2 %collective-permute-start.1 = (bf16[128,256]{1,0:T(8,128)(2,1)S(1)}, bf16[128,256]{1,0:T(8,128)(2,1)S(1)}, u32[]{:S(2)}, u32[]{:S(2)}) collective-permute-start(bf16[128,256]{1,0:T(8,128)(2,1)S(1)} %get-tuple-element.15), channel_id=1, source_target_pairs={{4,0},{8,4},{12,8},{16,12},{20,16},{24,20},{28,24},{5,1},{9,5},{13... | collective-permute-start | bytes 196616 | tf_op jit(solution)/shard_map/ppermute | solution.py:308
  67.3 4.1 %copy-start.6 = (bf16[128,256]{1,0:T(8,128)(2,1)}, bf16[128,256]{1,0:T(8,128)(2,1)S(1)}, u32[]{:S(2)}) copy-start(bf16[128,256]{1,0:T(8,128)(2,1)S(1)} %collective-permute-done.before) | copy-start | bytes 196612
  71.3 0.6 copy-start.7
Sparse Core Ops, SparseCore 0:
  8.9 31.2 all-gather.3
  46.0 60.8 all-gather.7
  109.9 59.7 all-gather.5
